TPU v7x, 32 devices: a whole 2x2x4 slice. The times are simulated.
32 devices in a mesh: rep: 2 (over x), fs: 4 (over z), tp: 4 (over y, core).
Axes of the slice: x: 2, y: 2, z: 4, core: 2. Of those that a mesh axis runs over, the one named last changes fastest.
Arguments:
- tokens: bfloat16 [4096, 2048], P(('rep', 'fs', 'tp')), may hold values from -6 to 6
- norm_gain: float32 [2048], replicated, may hold values from 0.1 to 1.9
- gate_weight: float32 [2048, 5632], P('fs', 'tp'), may hold values from -0.125 to 0.125
- gate_scale: float32 [5632], P('tp'), may hold values from 0.5 to 2
- up_weight: float32 [2048, 5632], P('fs', 'tp'), may hold values from -0.125 to 0.125
- up_scale: float32 [5632], P('tp'), may hold values from 0.5 to 2
- down_weight: float32 [5632, 2048], P('tp', 'fs'), may hold values from -0.078125 to 0.078125
- down_scale: float32 [2048], P('fs'), may hold values from 0.5 to 2
Outputs:
- mixed: bfloat16 [4096, 2048], P(('rep', 'fs', 'tp'))
All inputs are finite; a program needn't handle non-finite values.
Results may differ from a plain program's by a relative error of at most 0.014.
Values may be sent and summed in bfloat16 or wider, within the bound.
No kernel may reach another device: no remote copies, remote signals or barrier semaphores. Data moves between devices by JAX's collectives and lax.ppermute only.
A program may use at most 64 MiB of HBM per device.

v0:
```python
import jax
import jax.numpy as jnp
from jax import lax
from jax.sharding import PartitionSpec as P


def shards(
    tokens, norm_gain, gate_weight, gate_scale, up_weight, up_scale, down_weight, down_scale
):
    flat = tokens.astype(jnp.float32)
    mean_square = jnp.mean(flat * flat, axis=-1, keepdims=True)
    inverse = lax.rsqrt(mean_square + 1e-06)
    normed = (flat * inverse * norm_gain).astype(jnp.bfloat16)
    group = lax.all_gather(normed, "tp", axis=0, tiled=True)
    gate_low = gate_weight.astype(jnp.bfloat16)
    up_low = up_weight.astype(jnp.bfloat16)
    down_low = down_weight.astype(jnp.bfloat16)
    gate = jnp.dot(
        group,
        lax.all_gather(gate_low, "fs", axis=0, tiled=True),
        preferred_element_type=jnp.float32,
    )
    up = jnp.dot(
        group, lax.all_gather(up_low, "fs", axis=0, tiled=True), preferred_element_type=jnp.float32
    )
    down_full = lax.all_gather(down_low, "fs", axis=1, tiled=True)
    gate = gate * gate_scale
    up = up * up_scale
    hidden = (jax.nn.silu(gate) * up).astype(jnp.bfloat16)
    scales = lax.all_gather(down_scale, "fs", axis=0, tiled=True)
    total = lax.psum_scatter(
        jnp.dot(hidden, down_full, preferred_element_type=jnp.float32).astype(jnp.bfloat16),
        "tp",
        scatter_dimension=0,
        tiled=True,
    ).astype(jnp.float32)
    return (total * scales).astype(jnp.bfloat16)


def solution(mesh):
    in_specs = (
        P(("rep", "fs", "tp"), None),
        P(),
        P("fs", "tp"),
        P("tp"),
        P("fs", "tp"),
        P("tp"),
        P("tp", "fs"),
        P("fs"),
    )
    out_specs = P(("rep", "fs", "tp"), None)
    return jax.shard_map(shards, mesh=mesh, in_specs=in_specs, out_specs=out_specs, check_vma=False)
```

profile of v0, /device:TPU:0, one launch (start us, length us, event | category | flops | bytes accessed | tf_op | source)
XLA Modules:
  0.0 408.0 jit_solution(18322760977833249545)
XLA Ops:
  6.5 0.0 all-gather.6.cloned.1.call-start
  6.5 1.2 fusion.2
  7.8 2.0 fusion.4
  9.8 0.0 all-gather.6.cloned.1.call-update
  9.8 0.0 copy-start
  9.8 0.0 all-gather.8.cloned.1.call-start
  9.9 3.3 convert_element_type.29
  13.2 0.0 all-gather.8.cloned.1.call-update
  13.2 0.0 all-gather.10.cloned.1.call-start
  13.2 0.0 copy-done
  13.2 1.3 convert_element_type.30
  14.5 0.0 all-gather.10.cloned.1.call-update
  14.5 0.0 copy-start.3
  14.6 0.0 all-gather.12.cloned.1.call-start
  14.6 3.1 convert_element_type.32
  17.8 0.0 all-gather.12.cloned.1.call-update
  17.8 0.0 copy-start.4
  17.8 0.0 reduce-scatter.2.cloned.1.call-start
  17.8 17.4 %all-gather.6.cloned.1.call-done = bf16[512,2048]{1,0:T(8,128)(2,1)} async-done(((bf16[128,2048]{1,0:T(8,128)(2,1)}), bf16[512,2048]{1,0:T(8,128)(2,1)}) %all-gather.6.cloned.1.call-update) | async-done | bytes 2097168 | tf_op jit(solution)/shard_map/all_gather | solution.py:14
  35.3 0.0 copy-start.2
  35.3 108.3 %all-gather.8.cloned.1.call-done = bf16[2048,1408]{1,0:T(8,128)(2,1)} async-done(((bf16[512,1408]{1,0:T(8,128)(2,1)}), bf16[2048,1408]{1,0:T(8,128)(2,1)}) %all-gather.8.cloned.1.call-update) | async-done | bytes 5767184 | tf_op jit(solution)/shard_map/all_gather | solution.py:20
  143.6 0.0 copy-done.3
  143.6 8.2 %convolution_multiply_fusion.1 = f32[512,1408]{1,0:T(8,128)} fusion(bf16[512,2048]{1,0:T(8,128)(2,1)} %all-gather.6.cloned.1.call-done, bf16[2048,1408]{1,0:T(8,128)(2,1)} %all-gather.8.cloned.1.call-done, f32[1408]{0:T(1024)S(1)} %copy-done.3), kind=kOutput, calls=%fused_computation.2 | convolution fusion | flops 2953510912 | bytes 10753536 | tf_op jit(solution)/shard_map/dot_general | solution.py:18
  151.8 0.0 copy-start.1
  151.8 98.3 %all-gather.10.cloned.1.call-done = bf16[2048,1408]{1,0:T(8,128)(2,1)} async-done(((bf16[512,1408]{1,0:T(8,128)(2,1)}), bf16[2048,1408]{1,0:T(8,128)(2,1)}) %all-gather.10.cloned.1.call-update) | async-done | bytes 5767184 | tf_op jit(solution)/shard_map/all_gather | solution.py:24
  250.1 106.4 %all-gather.12.cloned.1.call-done = bf16[1408,2048]{1,0:T(8,128)(2,1)} async-done(((bf16[1408,512]{1,0:T(8,128)(2,1)}), bf16[1408,2048]{1,0:T(8,128)(2,1)}) %all-gather.12.cloned.1.call-update) | async-done | bytes 5767184 | tf_op jit(solution)/shard_map/all_gather | solution.py:26
  356.5 0.0 copy-done.4
  356.5 0.0 copy-done.2
  356.5 13.4 %convolution_convert_fusion = bf16[512,2048]{1,0:T(8,128)(2,1)} fusion(bf16[1408,2048]{1,0:T(8,128)(2,1)} %all-gather.12.cloned.1.call-done, bf16[512,2048]{1,0:T(8,128)(2,1)S(1)} %copy-done.2, bf16[2048,1408]{1,0:T(8,128)(2,1)} %all-gather.10.cloned.1.call-done, f32[512,1408]{1,0:T(8,128)} %convolution_multiply_fusion.1, f32[1408]{0:T(1024)S(1)} %copy-done.4), kind=kOutput, calls=%fused_computation.4 | convolution fusion | flops 5911674880 | bytes 18617856 | tf_op jit(solution)/shard_map/dot_general | solution.py:32
  370.0 0.0 reduce-scatter.2.cloned.1.call-update
  370.0 0.0 copy-done.1
  370.0 11.9 %all-gather = f32[4,1,512]{2,1,0:T(1,128)S(1)} all-gather(f32[1,1,512]{2,1,0:T(1,128)S(1)} %bitcast.8), channel_id=1, replica_groups=mesh['rep'=2,'fs'=4,'tp'=4] {'fs'}, dimensions={0}, use_global_device_ids=true | all-gather | bytes 10240 | tf_op jit(solution)/shard_map/all_gather | solution.py:30
  381.9 17.6 %reduce-scatter.2.cloned.1.call-done = bf16[128,2048]{1,0:T(8,128)(2,1)} async-done(((bf16[512,2048]{1,0:T(8,128)(2,1)}), bf16[128,2048]{1,0:T(8,128)(2,1)}) %reduce-scatter.2.cloned.1.call-update) | async-done | bytes 524304 | tf_op jit(solution)/shard_map/reduce_scatter | solution.py:31
  399.6 1.9 multiply_convert_fusion
  (1 shorter events, 0.0 us)
Async XLA Ops:
  6.5 28.7 %all-gather.6.cloned.1.call-start = ((), (), s32[]{:S(2)}) async-start(), calls=%async_computation.1 | async-start | bytes 2621440 | tf_op jit(solution)/shard_map/all_gather | solution.py:14
  9.8 3.4 copy-start
  9.8 133.7 %all-gather.8.cloned.1.call-start = ((), (), s32[]{:S(2)}) async-start(), calls=%async_computation.2 | async-start | bytes 7208960 | tf_op jit(solution)/shard_map/all_gather | solution.py:20
  13.2 236.9 %all-gather.10.cloned.1.call-start = ((), (), s32[]{:S(2)}) async-start(), calls=%async_computation.3 | async-start | bytes 7208960 | tf_op jit(solution)/shard_map/all_gather | solution.py:24
  14.5 129.0 %copy-start.3 = (f32[1408]{0:T(1024)S(1)}, f32[1408]{0:T(1024)}, u32[]{:S(2)}) copy-start(f32[1408]{0:T(1024)} %param.11) | copy-start | bytes 16900
  14.6 342.0 %all-gather.12.cloned.1.call-start = ((), (), s32[]{:S(2)}) async-start(), calls=%async_computation.4 | async-start | bytes 7208960 | tf_op jit(solution)/shard_map/all_gather | solution.py:26
  17.8 338.7 %copy-start.4 = (f32[1408]{0:T(1024)S(1)}, f32[1408]{0:T(1024)}, u32[]{:S(2)}) copy-start(f32[1408]{0:T(1024)} %param.13) | copy-start | bytes 16900
  17.8 381.8 %reduce-scatter.2.cloned.1.call-start = ((), (), s32[]{:S(2)}) async-start(), calls=%async_computation.5 | async-start | bytes 2621440 | tf_op jit(solution)/shard_map/reduce_scatter | solution.py:31
  35.3 321.2 %copy-start.2 = (bf16[512,2048]{1,0:T(8,128)(2,1)S(1)}, bf16[512,2048]{1,0:T(8,128)(2,1)}, u32[]{:S(2)}) copy-start(bf16[512,2048]{1,0:T(8,128)(2,1)} %all-gather.6.cloned.1.call-done) | copy-start | bytes 6291460
  151.8 218.2 %copy-start.1 = (f32[512]{0:T(512)S(1)}, f32[512]{0:T(512)}, u32[]{:S(2)}) copy-start(f32[512]{0:T(512)} %param.15) | copy-start | bytes 6148
Sparse Core Ops, SparseCore 0:
  9.9 25.2 all-gather.5
  36.8 106.6 all-gather.7
  145.1 104.9 all-gather.9
  251.5 104.9 all-gather.11
  370.1 29.4 reduce-scatter.1
where the time goes:
time: 408 us
  waiting for transfers between devices  348 us (85%)
  matrix products  21.7 us (5%)
  between operations  13.2 us (3%)
  other arithmetic  12.9 us (3%)
  blocking collectives  11.9 us (3%)
    all_gather x1, waiting for transfers between devices, shards(): lax.all_gather(gate_low, 'fs', axis=0, tiled=True)  108 us
    all_gather x1, waiting for transfers between devices, shards(): down_full = lax.all_gather(down_low, 'fs', axis=1, tiled=True)  106 us
    all_gather x1, waiting for transfers between devices, shards(): lax.all_gather(up_low, 'fs', axis=0, tiled=True)  98.3 us
    reduce_scatter x1, waiting for transfers between devices, shards(): lax.psum_scatter(jnp.dot(hidden, down_full, preferred_element_type=jnp.fl...  17.6 us
    all_gather x1, waiting for transfers between devices, shards(): group = lax.all_gather(normed, 'tp', axis=0, tiled=True)  17.4 us
    dot_general x1, matrix products, shards(): jnp.dot(hidden, down_full, preferred_element_type=jnp.float32)  13.4 us
    all_gather x1, blocking collectives, shards(): scales = lax.all_gather(down_scale, 'fs', axis=0, tiled=True)  11.9 us
    dot_general x1, matrix products, shards(): jnp.dot(group, lax.all_gather(gate_low, 'fs', axis=0, tiled=True), prefer...  8.23 us
  transfers between devices with their start and end apart: 5, of which 5 were waited for; matrix products, arithmetic and copies ran while one was open for 4% of the time, Pallas kernels for 0%

commit v1 on v0

--- a/solution.py
+++ b/solution.py
@@ -23,7 +23,9 @@
     up = jnp.dot(
         group, lax.all_gather(up_low, "fs", axis=0, tiled=True), preferred_element_type=jnp.float32
     )
-    down_full = lax.all_gather(down_low, "fs", axis=1, tiled=True)
+    down_full = jnp.concatenate(
+        lax.all_to_all(jnp.stack([down_low] * lax.axis_size("fs")), "fs", 0, 0), axis=1
+    )
     gate = gate * gate_scale
     up = up * up_scale
     hidden = (jax.nn.silu(gate) * up).astype(jnp.bfloat16)

time: 408 us -> 405 us (level)
  waiting for transfers between devices: 348 us -> 336 us
  starting transfers between devices: 0.17 us -> 6.7 us
    all_gather x1 -> x0, waiting for transfers between devices: 106 us -> none  [shards(): down_full = lax.all_gather(down_low, 'fs', axis=1, tiled=True)]
    all_gather x1, waiting for transfers between devices: 108 us -> 196 us  [shards(): lax.all_gather(gate_low, 'fs', axis=0, tiled=True)]
    all_gather x1, waiting for transfers between devices: 98.3 us -> 108 us  [shards(): lax.all_gather(up_low, 'fs', axis=0, tiled=True)]
    all_gather x1, waiting for transfers between devices: 17.4 us -> 8.6 us  [shards(): group = lax.all_gather(normed, 'tp', axis=0, tiled=True)]
    all_to_all x0 -> x1, starting transfers between devices: none -> 6.61 us  [shards(): lax.all_to_all(jnp.stack([down_low] * lax.axis_size('fs')), 'fs', 0, 0)]
    all_to_all x0 -> x1, waiting for transfers between devices: none -> 5.79 us  [shards(): lax.all_to_all(jnp.stack([down_low] * lax.axis_size('fs')), 'fs', 0, 0)]
  transfers between devices with their start and end apart: 5 -> 5, of which waited for: 5 -> 5; matrix products, arithmetic and copies ran while one was open for 4% -> 5% of each run, Pallas kernels for 0% -> 0%
where the time goes in v1:
time: 405 us
  waiting for transfers between devices  336 us (83%)
  matrix products  21.7 us (5%)
  between operations  13.2 us (3%)
  blocking collectives  11.9 us (3%)
  other arithmetic  11.5 us (3%)
  starting transfers between devices  6.7 us (2%)
    all_gather x1, waiting for transfers between devices, shards(): lax.all_gather(gate_low, 'fs', axis=0, tiled=True)  196 us
    all_gather x1, waiting for transfers between devices, shards(): lax.all_gather(up_low, 'fs', axis=0, tiled=True)  108 us
    reduce_scatter x1, waiting for transfers between devices, shards(): lax.psum_scatter(jnp.dot(hidden, down_full, preferred_element_type=jnp.fl...  17.6 us
    dot_general x1, matrix products, shards(): jnp.dot(hidden, down_full, preferred_element_type=jnp.float32)  13.4 us
    all_gather x1, blocking collectives, shards(): scales = lax.all_gather(down_scale, 'fs', axis=0, tiled=True)  11.9 us
    all_gather x1, waiting for transfers between devices, shards(): group = lax.all_gather(normed, 'tp', axis=0, tiled=True)  8.6 us
    dot_general x1, matrix products, shards(): jnp.dot(group, lax.all_gather(gate_low, 'fs', axis=0, tiled=True), prefer...  8.3 us
  transfers between devices with their start and end apart: 5, of which 5 were waited for; matrix products, arithmetic and copies ran while one was open for 5% of the time, Pallas kernels for 0%

profile of v1, /device:TPU:0, one launch (start us, length us, event | category | flops | bytes accessed | tf_op | source)
XLA Modules:
  0.0 404.6 jit_solution(12974803916923759330)
XLA Ops:
  6.5 0.0 all-gather.5.cloned.1.call-start
  6.5 1.2 fusion.2
  7.8 2.0 fusion.4
  9.8 0.0 all-gather.5.cloned.1.call-update
  9.8 0.0 all-gather.7.cloned.1.call-start
  9.9 3.1 convert_element_type.29
  12.9 0.0 all-gather.7.cloned.1.call-update
  13.0 2.0 convert_element_type.32
  15.0 0.8 copy.10
  15.8 2.9 stack.2
  18.7 0.0 copy-start
  18.7 6.6 %all-to-all-start = ((bf16[4,1408,512]{1,2,0:T(8,128)(2,1)}), bf16[4,1408,512]{1,2,0:T(8,128)(2,1)}, u32[]{:S(2)}, u32[]{:S(2)}) async-start(bf16[4,1408,512]{1,2,0:T(8,128)(2,1)} %stack.2), calls=%async_computation | async-start | bytes 11534336 | tf_op jit(solution)/shard_map/all_to_all | solution.py:27
  25.3 0.0 copy-start.3
  25.3 0.0 all-gather.9.cloned.1.call-start
  25.3 0.0 copy-done
  25.3 1.3 convert_element_type.30
  26.6 0.0 all-gather.9.cloned.1.call-update
  26.6 0.0 copy-start.4
  26.6 0.0 reduce-scatter.2.cloned.1.call-start
  26.7 8.6 %all-gather.5.cloned.1.call-done = bf16[512,2048]{1,0:T(8,128)(2,1)} async-done(((bf16[128,2048]{1,0:T(8,128)(2,1)}), bf16[512,2048]{1,0:T(8,128)(2,1)}) %all-gather.5.cloned.1.call-update) | async-done | bytes 2097168 | tf_op jit(solution)/shard_map/all_gather | solution.py:14
  35.3 0.0 copy-start.2
  35.3 196.1 %all-gather.7.cloned.1.call-done = bf16[2048,1408]{1,0:T(8,128)(2,1)} async-done(((bf16[512,1408]{1,0:T(8,128)(2,1)}), bf16[2048,1408]{1,0:T(8,128)(2,1)}) %all-gather.7.cloned.1.call-update) | async-done | bytes 5767184 | tf_op jit(solution)/shard_map/all_gather | solution.py:20
  231.3 0.0 copy-done.3
  231.3 8.3 %convolution_multiply_fusion.1 = f32[512,1408]{1,0:T(8,128)} fusion(bf16[512,2048]{1,0:T(8,128)(2,1)} %all-gather.5.cloned.1.call-done, bf16[2048,1408]{1,0:T(8,128)(2,1)} %all-gather.7.cloned.1.call-done, f32[1408]{0:T(1024)S(1)} %copy-done.3), kind=kOutput, calls=%fused_computation.2 | convolution fusion | flops 2953510912 | bytes 10753536 | tf_op jit(solution)/shard_map/dot_general | solution.py:18
  239.6 5.8 %all-to-all-done = bf16[4,1408,512]{1,2,0:T(8,128)(2,1)} async-done(((bf16[4,1408,512]{1,2,0:T(8,128)(2,1)}), bf16[4,1408,512]{1,2,0:T(8,128)(2,1)}, u32[]{:S(2)}, u32[]{:S(2)}) %all-to-all-start) | async-done | bytes 5767200 | tf_op jit(solution)/shard_map/all_to_all | solution.py:27
  245.4 107.7 %all-gather.9.cloned.1.call-done = bf16[2048,1408]{1,0:T(8,128)(2,1)} async-done(((bf16[512,1408]{1,0:T(8,128)(2,1)}), bf16[2048,1408]{1,0:T(8,128)(2,1)}) %all-gather.9.cloned.1.call-update) | async-done | bytes 5767184 | tf_op jit(solution)/shard_map/all_gather | solution.py:24
  353.1 0.0 copy-done.4
  353.1 0.0 copy-done.2
  353.1 0.0 copy-start.1
  353.1 13.4 %convolution_convert_fusion = bf16[512,2048]{1,0:T(8,128)(2,1)} fusion(bf16[1408,2048]{0,1:T(8,128)(2,1)} %bitcast.1, bf16[512,2048]{1,0:T(8,128)(2,1)S(1)} %copy-done.2, bf16[2048,1408]{1,0:T(8,128)(2,1)} %all-gather.9.cloned.1.call-done, f32[512,1408]{1,0:T(8,128)} %convolution_multiply_fusion.1, f32[1408]{0:T(1024)S(1)} %copy-done.4), kind=kOutput, calls=%fused_computation.4 | convolution fusion | flops 5911674880 | bytes 18617856 | tf_op jit(solution)/shard_map/dot_general | solution.py:34
  366.5 0.0 reduce-scatter.2.cloned.1.call-update
  366.6 0.0 copy-done.1
  366.6 11.9 %all-gather = f32[4,1,512]{2,1,0:T(1,128)S(1)} all-gather(f32[1,1,512]{2,1,0:T(1,128)S(1)} %bitcast.11), channel_id=1, replica_groups=mesh['rep'=2,'fs'=4,'tp'=4] {'fs'}, dimensions={0}, use_global_device_ids=true | all-gather | bytes 10240 | tf_op jit(solution)/shard_map/all_gather | solution.py:32
  378.5 17.6 %reduce-scatter.2.cloned.1.call-done = bf16[128,2048]{1,0:T(8,128)(2,1)} async-done(((bf16[512,2048]{1,0:T(8,128)(2,1)}), bf16[128,2048]{1,0:T(8,128)(2,1)}) %reduce-scatter.2.cloned.1.call-update) | async-done | bytes 524304 | tf_op jit(solution)/shard_map/reduce_scatter | solution.py:33
  396.2 1.9 multiply_convert_fusion
  (1 shorter events, 0.0 us)
Async XLA Ops:
  6.5 28.7 %all-gather.5.cloned.1.call-start = ((), (), s32[]{:S(2)}) async-start(), calls=%async_computation.2 | async-start | bytes 2621440 | tf_op jit(solution)/shard_map/all_gather | solution.py:14
  9.8 221.5 %all-gather.7.cloned.1.call-start = ((), (), s32[]{:S(2)}) async-start(), calls=%async_computation.3 | async-start | bytes 7208960 | tf_op jit(solution)/shard_map/all_gather | solution.py:20
  18.7 6.6 %copy-start = (f32[512,1408]{1,0:T(8,128)S(1)}, f32[512,1408]{1,0:T(8,128)}, u32[]{:S(2)}) copy-start(f32[512,1408]{1,0:T(8,128)} %param.12) | copy-start | bytes 8650756
  18.7 226.7 %all-to-all-start = ((bf16[4,1408,512]{1,2,0:T(8,128)(2,1)}), bf16[4,1408,512]{1,2,0:T(8,128)(2,1)}, u32[]{:S(2)}, u32[]{:S(2)}) async-start(bf16[4,1408,512]{1,2,0:T(8,128)(2,1)} %stack.2), calls=%async_computation | async-start | bytes 11534336 | tf_op jit(solution)/shard_map/all_to_all | solution.py:27
  25.3 206.0 %copy-start.3 = (f32[1408]{0:T(1024)S(1)}, f32[1408]{0:T(1024)}, u32[]{:S(2)}) copy-start(f32[1408]{0:T(1024)} %param.11) | copy-start | bytes 16900
  25.3 327.8 %all-gather.9.cloned.1.call-start = ((), (), s32[]{:S(2)}) async-start(), calls=%async_computation.4 | async-start | bytes 7208960 | tf_op jit(solution)/shard_map/all_gather | solution.py:24
  26.6 326.5 %copy-start.4 = (f32[1408]{0:T(1024)S(1)}, f32[1408]{0:T(1024)}, u32[]{:S(2)}) copy-start(f32[1408]{0:T(1024)} %param.13) | copy-start | bytes 16900
  26.6 369.5 %reduce-scatter.2.cloned.1.call-start = ((), (), s32[]{:S(2)}) async-start(), calls=%async_computation.5 | async-start | bytes 2621440 | tf_op jit(solution)/shard_map/reduce_scatter | solution.py:33
  35.3 317.8 %copy-start.2 = (bf16[512,2048]{1,0:T(8,128)(2,1)S(1)}, bf16[512,2048]{1,0:T(8,128)(2,1)}, u32[]{:S(2)}) copy-start(bf16[512,2048]{1,0:T(8,128)(2,1)} %all-gather.5.cloned.1.call-done) | copy-start | bytes 6291460
  353.1 13.4 %copy-start.1 = (f32[512]{0:T(512)S(1)}, f32[512]{0:T(512)}, u32[]{:S(2)}) copy-start(f32[512]{0:T(512)} %param.15) | copy-start | bytes 6148
Sparse Core Ops, SparseCore 0:
  9.9 25.2 all-gather.4
  36.8 194.4 all-gather.6
  232.9 120.1 all-gather.8
  366.7 29.4 reduce-scatter.1
